TPU v7x, 32 devices: a whole 2x2x4 slice. The times are simulated.
32 devices in a mesh: ep: 8 (over z, x), tp: 4 (over y, core).
Axes of the slice: x: 2, y: 2, z: 4, core: 2. Of those that a mesh axis runs over, the one named last changes fastest.
Arguments:
- tokens: bfloat16 [1024, 2048], P('ep'), may hold values from -6 to 6
- cotangent: bfloat16 [1024, 2048], P('ep'), may hold values from -1.5 to 1.5
- routes: int32 [1024, 2], P('ep'), may hold values from 0 to 3, all different within a row; in each aligned block of 128 rows (0 to 127, 128 to 255, ...) at most 96 rows name the same one
- router: bfloat16 [2048, 4], replicated, may hold values from -0.125 to 0.125
- w_gate: bfloat16 [8, 2048, 2048], P('ep', None, 'tp'), may hold values from -0.125 to 0.125
- w_up: bfloat16 [8, 2048, 2048], P('ep', None, 'tp'), may hold values from -0.125 to 0.125
- w_down: bfloat16 [8, 2048, 2048], P('ep', 'tp'), may hold values from -0.09375 to 0.09375
Outputs:
- token_grad: bfloat16 [1024, 2048], P('ep', 'tp')
- gate_grad: float32 [1024, 2], P('ep')
- grad_gate: bfloat16 [8, 2048, 2048], P('ep', None, 'tp')
- grad_up: bfloat16 [8, 2048, 2048], P('ep', None, 'tp')
- grad_down: bfloat16 [8, 2048, 2048], P('ep', 'tp')
- router_grad: float32 [2048, 4], P(('ep', 'tp'))
Inputs may be any that keep to these rules, and one draw needn't show every extreme that they name: `routes`: each row names 2 different experts. In the rows of one index of ep (aligned blocks of 128 rows) no expert is named by more than 96 rows, a bound that some block reaches.
All inputs are finite; a program needn't handle non-finite values.
Results may differ from a plain program's by a relative error of at most 0.018.
Values may be sent and summed in bfloat16 or wider, within the bound.
No kernel may reach another device: no remote copies, remote signals or barrier semaphores. Data moves between devices by JAX's collectives and lax.ppermute only.
A program may use at most 64 MiB of HBM per device.

v0:
```python
import jax
import jax.numpy as jnp
from jax import lax
from jax.sharding import PartitionSpec as P

BLOCKS = 2


def build_slots(block_routes, experts, capacity):
    flat_routes = block_routes.reshape(-1)
    labels = jnp.arange(experts, dtype=jnp.int32)
    hit_mask = (flat_routes[None, :] == labels[:, None]).astype(jnp.int32)
    rank_in = jnp.cumsum(hit_mask, axis=1, dtype=jnp.int32) - 1
    slot_ids = jnp.arange(capacity, dtype=jnp.int32)
    assigned = (hit_mask[:, None, :] == 1) & (rank_in[:, None, :] == slot_ids[None, :, None])
    return assigned.astype(jnp.float32)


def gate_pair(tokens, routes, router, experts):
    logits = jnp.dot(tokens, router, preferred_element_type=jnp.float32)
    labels = jnp.arange(experts, dtype=jnp.int32)
    picked = (routes[:, :, None] == labels[None, None, :]).astype(jnp.float32)
    chosen = jnp.sum(picked * logits[:, None, :], axis=2)
    margin = chosen[:, 0] - chosen[:, 1]
    weights = jnp.stack([jax.nn.sigmoid(margin), jax.nn.sigmoid(-margin)], axis=1)
    return (picked, weights)


def logit_grads(picked, weights, gate_grad):
    lead_grad = weights[:, 0] * weights[:, 1] * (gate_grad[:, 0] - gate_grad[:, 1])
    pair_grad = jnp.stack([lead_grad, -lead_grad], axis=1)
    return jnp.sum(picked * pair_grad[:, :, None], axis=1)


def expert_grads(rows_in, cot_in, gate_in, gate_weight, up_weight, down_weight):
    pre_gate = jnp.dot(rows_in, gate_weight, preferred_element_type=jnp.float32)
    pre_up = jnp.dot(rows_in, up_weight, preferred_element_type=jnp.float32)
    back_grad = lax.dot_general(
        cot_in, down_weight, (((1,), (1,)), ((), ())), preferred_element_type=jnp.float32
    )
    sig_gate = jax.nn.sigmoid(pre_gate)
    active = pre_gate * sig_gate
    hidden = (active * pre_up).astype(jnp.bfloat16)
    gate_terms = jnp.sum(hidden.astype(jnp.float32) * back_grad, axis=1)
    gate_col = gate_in.astype(jnp.float32)[:, None]
    scaled_back = gate_col * back_grad
    d_gate = (scaled_back * pre_up * sig_gate * (1.0 + pre_gate * (1.0 - sig_gate))).astype(
        jnp.bfloat16
    )
    d_up = (scaled_back * active).astype(jnp.bfloat16)
    scaled_cot = (gate_col * cot_in.astype(jnp.float32)).astype(jnp.bfloat16)
    contract_rows = (((0,), (0,)), ((), ()))
    grad_gate = lax.dot_general(
        rows_in, d_gate, contract_rows, preferred_element_type=jnp.float32
    ).astype(jnp.bfloat16)
    grad_up = lax.dot_general(
        rows_in, d_up, contract_rows, preferred_element_type=jnp.float32
    ).astype(jnp.bfloat16)
    grad_down = lax.dot_general(
        hidden, scaled_cot, contract_rows, preferred_element_type=jnp.float32
    ).astype(jnp.bfloat16)
    return (d_gate, d_up, gate_terms, grad_gate, grad_up, grad_down)


def spread_slabs(packed, experts, slab_count):
    widened = jnp.broadcast_to(packed[:, None], (experts, BLOCKS) + packed.shape[1:])
    return widened.reshape((slab_count,) + packed.shape[1:])


def shards(tokens, cotangent, routes, router, w_gate, w_up, w_down):
    highest = lax.Precision.HIGHEST
    ep_count = lax.axis_size("ep")
    tp_count = lax.axis_size("tp")
    experts = ep_count // BLOCKS
    tok_rows, width = tokens.shape
    top_count = routes.shape[1]
    capacity = 3 * tok_rows * top_count // (2 * experts)
    col_width = width // tp_count
    tp_index = lax.axis_index("tp")
    picked, weights = gate_pair(tokens, routes, router, experts)
    assigned = build_slots(routes, experts, capacity)
    per_token = jnp.sum(assigned.reshape(experts, capacity, tok_rows, top_count), axis=3)
    token_map = per_token.astype(jnp.bfloat16)
    gate_send = weights.astype(jnp.bfloat16)
    gate_slots = jnp.einsum(
        "ecj,j->ec", assigned, gate_send.astype(jnp.float32).reshape(-1), precision=highest
    ).astype(jnp.bfloat16)
    gate_out = spread_slabs(gate_slots, experts, ep_count)

    def pack_rows(source):
        packed = jnp.einsum(
            "ect,td->ecd", token_map, source, preferred_element_type=jnp.float32
        ).astype(jnp.bfloat16)
        return spread_slabs(packed, experts, ep_count)

    tok_part = lax.dynamic_slice_in_dim(tokens, tp_index * col_width, col_width, 1)
    cot_part = lax.dynamic_slice_in_dim(cotangent, tp_index * col_width, col_width, 1)
    recv_part, recv_cot_part, recv_gate = (
        lax.all_to_all(pack_rows(tok_part), "ep", split_axis=0, concat_axis=0, tiled=True),
        lax.all_to_all(pack_rows(cot_part), "ep", split_axis=0, concat_axis=0, tiled=True),
        lax.all_to_all(gate_out, "ep", split_axis=0, concat_axis=0, tiled=True),
    )
    recv_rows, recv_cot = (
        lax.all_gather(recv_part, "tp", axis=2, tiled=True),
        lax.all_gather(recv_cot_part, "tp", axis=2, tiled=True),
    )
    rows_in = recv_rows.reshape(-1, width)
    cot_in = recv_cot.reshape(-1, width)
    gate_in = recv_gate.reshape(-1)
    d_gate, d_up, gate_terms, grad_gate, grad_up, grad_down = expert_grads(
        rows_in, cot_in, gate_in, w_gate[0], w_up[0], w_down[0]
    )
    contract_hidden = (((1,), (1,)), ((), ()))
    partial_dx = lax.dot_general(
        d_gate, w_gate[0], contract_hidden, preferred_element_type=jnp.float32
    )
    partial_dx = partial_dx + lax.dot_general(
        d_up, w_up[0], contract_hidden, preferred_element_type=jnp.float32
    )
    summed_dx = lax.psum_scatter(
        partial_dx.reshape(ep_count, capacity, width).astype(jnp.bfloat16),
        "tp",
        scatter_dimension=2,
        tiled=True,
    ).astype(jnp.float32)
    gate_sums = lax.psum(gate_terms.reshape(ep_count, capacity), "tp")
    back_dx, back_gate = (
        lax.all_to_all(
            summed_dx.astype(jnp.bfloat16), "ep", split_axis=0, concat_axis=0, tiled=True
        ).astype(summed_dx.dtype),
        lax.all_to_all(
            gate_sums.astype(jnp.bfloat16), "ep", split_axis=0, concat_axis=0, tiled=True
        ).astype(gate_sums.dtype),
    )
    slab_dx = jnp.sum(back_dx.reshape(experts, BLOCKS, capacity, col_width), axis=1)
    routed_dx = jnp.einsum("ect,ecd->td", per_token, slab_dx, precision=highest)
    slab_gate = jnp.sum(back_gate.reshape(experts, BLOCKS, capacity), axis=1)
    gate_grad = jnp.einsum("ecj,ec->j", assigned, slab_gate, precision=highest).reshape(
        tok_rows, top_count
    )
    logit_grad = logit_grads(picked, weights, gate_grad)
    router_cols = lax.dynamic_slice_in_dim(router, tp_index * col_width, col_width, 0).astype(
        jnp.float32
    )
    token_grad = (routed_dx + jnp.dot(logit_grad, router_cols.T, precision=highest)).astype(
        jnp.bfloat16
    )
    seg_rows = tok_rows // tp_count
    own_rows = lax.dynamic_slice_in_dim(tokens, tp_index * seg_rows, seg_rows, 0).astype(
        jnp.float32
    )
    own_logit = lax.dynamic_slice_in_dim(logit_grad, tp_index * seg_rows, seg_rows, 0)
    router_grad = lax.psum_scatter(
        jnp.dot(own_rows.T, own_logit, precision=highest),
        ("ep", "tp"),
        scatter_dimension=0,
        tiled=True,
    )
    return (token_grad, gate_grad, grad_gate[None], grad_up[None], grad_down[None], router_grad)


def solution(mesh):
    placed = (
        P("ep", None),
        P("ep", None),
        P("ep", None),
        P(),
        P("ep", None, "tp"),
        P("ep", None, "tp"),
        P("ep", "tp", None),
    )
    return jax.shard_map(
        shards,
        mesh=mesh,
        in_specs=placed,
        out_specs=(
            P("ep", "tp"),
            P("ep", None),
            P("ep", None, "tp"),
            P("ep", None, "tp"),
            P("ep", "tp", None),
            P(("ep", "tp"), None),
        ),
        check_vma=False,
    )
```

profile of v0, /device:TPU:0, one launch (start us, length us, event | category | flops | bytes accessed | tf_op | source)
XLA Modules:
  0.0 325.1 jit_solution(1084350082928045645)
XLA Ops:
  8.3 1.2 reduce-window.6
  12.1 27.3 %all_to_all.33 = bf16[8,96,512]{2,1,0:T(8,128)(2,1)} all-to-all(bf16[8,96,512]{2,1,0:T(8,128)(2,1)S(1)} %bitcast.80), channel_id=1, replica_groups=mesh['ep'=8,'tp'=4] {'ep'}, dimensions={0} | all-to-all | bytes 1572864 | tf_op jit(solution)/shard_map/all_to_all | solution.py:99
  39.5 1.2 convolution_convert_fusion.3
  40.8 23.3 %all_to_all.34 = bf16[8,96,512]{2,1,0:T(8,128)(2,1)} all-to-all(bf16[8,96,512]{2,1,0:T(8,128)(2,1)S(1)} %bitcast.81), channel_id=1, replica_groups=mesh['ep'=8,'tp'=4] {'ep'}, dimensions={0} | all-to-all | bytes 1572864 | tf_op jit(solution)/shard_map/all_to_all | solution.py:100
  64.7 2.4 all-gather.5.cloned.1.call-done
  67.1 5.7 %fusion.11 = f32[768,512]{0,1:T(8,128)} fusion(bf16[768,2048]{1,0:T(8,128)(2,1)} %bitcast.95, bf16[1,2048,512]{2,1,0:T(8,128)(2,1)} %param.12), kind=kOutput, calls=%fused_computation.15 | convolution fusion | flops 1610612736 | bytes 6815744 | tf_op jit(solution)/shard_map/dot_general | solution.py:37
  72.8 3.0 fusion.8
  75.8 21.4 %all-gather.3.cloned.1.call-done = bf16[8,96,2048]{2,1,0:T(8,128)(2,1)} async-done(((bf16[8,96,512]{2,1,0:T(8,128)(2,1)}), bf16[8,96,2048]{2,1,0:T(8,128)(2,1)}) %all-gather.3.cloned.1.call-update) | async-done | bytes 3145744 | tf_op jit(solution)/shard_map/all_gather | solution.py:105
  97.2 6.7 %multiply_reduce_fusion = (f32[768]{0:T(1024)S(1)}, bf16[768,512]{0,1:T(8,128)(2,1)}, f32[768,512]{0,1:T(8,128)}) fusion(f32[768,512]{0,1:T(8,128)} %fusion.11, f32[768,512]{0,1:T(8,128)} %fusion.8, bf16[768,2048]{1,0:T(8,128)(2,1)} %bitcast.99, bf16[1,512,2048]{2,1,0:T(8,128)(2,1)} %param.13), kind=kOutput, calls=%fused_computation.20 | convolution fusion | flops 1614150912 | bytes 10750976 | tf_op jit(solution)/shard_map/dot_general | solution.py:38
  104.1 5.9 %psum.7 = bf16[8,96]{1,0:T(8,128)(2,1)S(1)} all-reduce(f32[8,96]{1,0:T(8,128)S(1)} %reshape.150), channel_id=1, replica_groups=mesh['ep'=8,'tp'=4] {'tp'}, use_global_device_ids=true, to_apply=%region_7.8 | all-reduce | flops 768 | bytes 4608 | tf_op jit(solution)/shard_map/psum | solution.py:126
  110.5 5.7 %all-to-all-start.4 = ((bf16[8,1,96]{2,1,0:T(2,128)(2,1)}), bf16[8,1,96]{2,1,0:T(2,128)(2,1)S(1)}, u32[]{:S(2)}, u32[]{:S(2)}) async-start(bf16[8,1,96]{2,1,0:T(2,128)(2,1)} %copy.80), calls=%async_computation.5 | async-start | bytes 8192 | tf_op jit(solution)/shard_map/all_to_all | solution.py:131
  116.5 6.1 %all-to-all-done.4 = bf16[8,1,96]{2,1,0:T(2,128)(2,1)S(1)} async-done(((bf16[8,1,96]{2,1,0:T(2,128)(2,1)}), bf16[8,1,96]{2,1,0:T(2,128)(2,1)S(1)}, u32[]{:S(2)}, u32[]{:S(2)}) %all-to-all-start.4) | async-done | bytes 1568 | tf_op jit(solution)/shard_map/all_to_all | solution.py:131
  123.4 8.9 %all_to_all.35 = bf16[8,1,96]{2,1,0:T(2,128)(2,1)S(1)} all-to-all(bf16[8,1,96]{2,1,0:T(2,128)(2,1)S(1)} %copy.77), channel_id=1, replica_groups=mesh['ep'=8,'tp'=4] {'ep'}, dimensions={0} | all-to-all | bytes 3072 | tf_op jit(solution)/shard_map/all_to_all | solution.py:101
  132.4 3.1 multiply_convert_fusion.7
  135.5 1.8 fusion.6
  137.7 3.5 %add_convert_fusion = bf16[768,2048]{1,0:T(8,128)(2,1)} fusion(f32[768,2048]{1,0:T(8,128)S(1)} %fusion.6, bf16[768,512]{0,1:T(8,128)(2,1)S(1)} %get-tuple-element.12, bf16[1,2048,512]{2,1,0:T(8,128)(2,1)S(1)} %copy-done.4), kind=kOutput, calls=%fused_computation.1 | convolution fusion | flops 1613758464 | bytes 12320768 | tf_op jit(solution)/shard_map/dot_general | solution.py:117
  141.4 1.8 fusion.31
  143.2 33.2 %reduce-scatter.5.cloned.1.call-done = bf16[8,96,512]{2,1,0:T(8,128)(2,1)} async-done(((bf16[8,96,2048]{2,1,0:T(8,128)(2,1)}), bf16[8,96,512]{2,1,0:T(8,128)(2,1)}) %reduce-scatter.5.cloned.1.call-update) | async-done | bytes 786448 | tf_op jit(solution)/shard_map/reduce_scatter | solution.py:120
  176.4 5.5 %all-to-all-start.3 = ((bf16[8,96,512]{2,1,0:T(8,128)(2,1)}), bf16[8,96,512]{2,1,0:T(8,128)(2,1)S(1)}, u32[]{:S(2)}, u32[]{:S(2)}) async-start(bf16[8,96,512]{2,1,0:T(8,128)(2,1)} %reduce-scatter.5.cloned.1.call-done), calls=%async_computation.4 | async-start | bytes 1572864 | tf_op jit(solution)/shard_map/all_to_all | solution.py:128
  181.9 5.4 %fusion.3 = bf16[1,2048,512]{2,1,0:T(8,128)(2,1)} fusion(bf16[768,2048]{1,0:T(8,128)(2,1)} %bitcast.96, bf16[768,512]{0,1:T(8,128)(2,1)} %copy-done.3), kind=kOutput, calls=%fused_computation.7 | convolution fusion | flops 1611661312 | bytes 6029312 | tf_op jit(solution)/shard_map/dot_general | solution.py:53
  187.3 3.2 fusion.5
  190.6 3.2 fusion.4
  193.8 121.5 %reduce-scatter.7.cloned.1.call-done = f32[64,4]{1,0:T(8,128)} async-done(((f32[2048,4]{1,0:T(8,128)}), f32[64,4]{1,0:T(8,128)}) %reduce-scatter.7.cloned.1.call-update) | async-done | bytes 1040
  315.3 1.4 copy.85
  (81 shorter events, 8.4 us)
Async XLA Ops:
  7.2 65.6 %copy-start = (bf16[1,2048,512]{2,1,0:T(8,128)(2,1)S(1)}, bf16[1,2048,512]{2,1,0:T(8,128)(2,1)}, u32[]{:S(2)}) copy-start(bf16[1,2048,512]{2,1,0:T(8,128)(2,1)} %param.11) | copy-start | bytes 6291460
  7.2 60.0 %all-gather.5.cloned.1.call-start = ((), (), s32[]{:S(2)}) async-start(), calls=%async_computation.8 | async-start | bytes 3932160 | tf_op jit(solution)/shard_map/all_gather | solution.py:104
  39.4 24.9 %copy-start.7 = (s32[128,2]{0,1:T(2,128)S(1)}, s32[128,2]{0,1:T(2,128)}, u32[]{:S(2)}) copy-start(s32[128,2]{0,1:T(2,128)} %param.9) | copy-start | bytes 3076
  39.5 25.0 %copy-start.5 = (bf16[128,2048]{1,0:T(8,128)(2,1)S(1)}, bf16[128,2048]{1,0:T(8,128)(2,1)}, u32[]{:S(2)}) copy-start(bf16[128,2048]{1,0:T(8,128)(2,1)} %param.7) | copy-start | bytes 1572868
  39.5 25.0 %copy-start.6 = (bf16[2048,4]{0,1:T(4,128)(2,1)S(1)}, bf16[2048,4]{0,1:T(4,128)(2,1)}, u32[]{:S(2)}) copy-start(bf16[2048,4]{0,1:T(4,128)(2,1)} %param.10) | copy-start | bytes 49156
  39.5 57.8 %all-gather.3.cloned.1.call-start = ((), (), s32[]{:S(2)}) async-start(), calls=%async_computation.7 | async-start | bytes 3932160 | tf_op jit(solution)/shard_map/all_gather | solution.py:105
  67.1 5.7 %copy-start.9 = (bf16[8,96,2048]{2,1,0:T(8,128)(2,1)S(1)}, bf16[8,96,2048]{2,1,0:T(8,128)(2,1)}, u32[]{:S(2)}) copy-start(bf16[8,96,2048]{2,1,0:T(8,128)(2,1)} %all-gather.5.cloned.1.call-done) | copy-start | bytes 9437188
  110.5 12.1 %all-to-all-start.4 = ((bf16[8,1,96]{2,1,0:T(2,128)(2,1)}), bf16[8,1,96]{2,1,0:T(2,128)(2,1)S(1)}, u32[]{:S(2)}, u32[]{:S(2)}) async-start(bf16[8,1,96]{2,1,0:T(2,128)(2,1)} %copy.80), calls=%async_computation.5 | async-start | bytes 8192 | tf_op jit(solution)/shard_map/all_to_all | solution.py:131
  116.2 60.2 %reduce-scatter.5.cloned.1.call-start = ((), (), s32[]{:S(2)}) async-start(), calls=%async_computation.9 | async-start | bytes 3932160 | tf_op jit(solution)/shard_map/reduce_scatter | solution.py:120
  122.8 12.7 %copy-start.8 = (f32[1,128,2,1]{1,0,3,2:T(1,128)}, f32[1,128,2,1]{1,0,3,2:T(1,128)S(1)}, u32[]{:S(2)}) copy-start(f32[1,128,2,1]{1,0,3,2:T(1,128)S(1)} %fusion.23) | copy-start | bytes 3076
  135.5 1.9 copy-start.3
  135.5 1.9 copy-start.1
  135.5 2.2 copy-start.4
  141.3 174.1 %reduce-scatter.7.cloned.1.call-start = ((), (), s32[]{:S(2)}) async-start(), calls=%async_computation.10 | async-start | bytes 1081344
  176.4 140.3 %all-to-all-start.3 = ((bf16[8,96,512]{2,1,0:T(8,128)(2,1)}), bf16[8,96,512]{2,1,0:T(8,128)(2,1)S(1)}, u32[]{:S(2)}, u32[]{:S(2)}) async-start(bf16[8,96,512]{2,1,0:T(8,128)(2,1)} %reduce-scatter.5.cloned.1.call-done), calls=%async_computation.4 | async-start | bytes 1572864 | tf_op jit(solution)/shard_map/all_to_all | solution.py:128
  181.9 5.4 %copy-start.11 = (bf16[8,96,2048]{2,1,0:T(8,128)(2,1)S(1)}, bf16[8,96,2048]{2,1,0:T(8,128)(2,1)}, u32[]{:S(2)}) copy-start(bf16[8,96,2048]{2,1,0:T(8,128)(2,1)} %all-gather.3.cloned.1.call-done) | copy-start | bytes 9437188
  181.9 5.4 %copy-start.12 = (bf16[768,512]{0,1:T(8,128)(2,1)S(1)}, bf16[768,512]{0,1:T(8,128)(2,1)}, u32[]{:S(2)}) copy-start(bf16[768,512]{0,1:T(8,128)(2,1)} %get-tuple-element.11) | copy-start | bytes 2359300
  187.3 3.3 %copy-start.2 = (bf16[768,512]{0,1:T(8,128)(2,1)S(1)}, bf16[768,512]{0,1:T(8,128)(2,1)}, u32[]{:S(2)}) copy-start(bf16[768,512]{0,1:T(8,128)(2,1)} %copy-done.1) | copy-start | bytes 2359300
  187.3 3.3 %copy-start.10 = (bf16[8,96,2048]{2,1,0:T(8,128)(2,1)S(1)}, bf16[8,96,2048]{2,1,0:T(8,128)(2,1)}, u32[]{:S(2)}) copy-start(bf16[8,96,2048]{2,1,0:T(8,128)(2,1)} %all-gather.5.cloned.1.call-done) | copy-start | bytes 9437188
Sparse Core Ops, SparseCore 0:
  39.6 27.5 all-gather.4
  68.7 28.4 all-gather.2
  141.4 34.9 reduce-scatter.4
  178.5 136.7 reduce-scatter.6
where the time goes:
time: 326 us; the launch traced here: 325 us
  waiting for transfers between devices  185 us (57%)
  blocking collectives  65.4 us (20%)
  matrix products  39.1 us (12%)
  between operations  14.1 us (4%)
  starting transfers between devices  11.3 us (3%)
  other arithmetic  5.65 us (2%)
  local copies, waits for them, and re-layouts  4.82 us (1%)
    unnamed x5, waiting for transfers between devices  122 us
    reduce_scatter x1, waiting for transfers between devices, shards(): lax.psum_scatter(partial_dx.reshape(ep_count, capacity, width).astype(jnp...  33.2 us
    all_to_all x1, blocking collectives, shards(): lax.all_to_all(pack_rows(tok_part), 'ep', split_axis=0, concat_axis=0, ti...  27.3 us
    all_to_all x1, blocking collectives, shards(): lax.all_to_all(pack_rows(cot_part), 'ep', split_axis=0, concat_axis=0, ti...  23.3 us
    all_gather x1, waiting for transfers between devices, shards(): lax.all_gather(recv_cot_part, 'tp', axis=2, tiled=True)  21.4 us
    all_to_all x1, blocking collectives, shards(): lax.all_to_all(gate_out, 'ep', split_axis=0, concat_axis=0, tiled=True)  8.86 us
    dot_general x1, matrix products, expert_grads(): lax.dot_general(cot_in, down_weight, (((1,), (1,)), ((), ())), preferred_...  6.74 us
  transfers between devices with their start and end apart: 6, of which 5 were waited for; matrix products, arithmetic and copies ran while one was open for 8% of the time, Pallas kernels for 0%

commit v1 on v0

--- a/solution.py
+++ b/solution.py
@@ -2,8 +2,14 @@
 import jax.numpy as jnp
 from jax import lax
 from jax.sharding import PartitionSpec as P
+from jax.lax import all_gather
 
 BLOCKS = 2
+
+
+def serve_stacks_all_on(in_array, shard_axis):
+    taken_in = all_gather(in_array, axis_name=shard_axis)
+    return jnp.concatenate(taken_in, axis=2)
 
 
 def build_slots(block_routes, experts, capacity):
@@ -102,7 +108,7 @@
     )
     recv_rows, recv_cot = (
         lax.all_gather(recv_part, "tp", axis=2, tiled=True),
-        lax.all_gather(recv_cot_part, "tp", axis=2, tiled=True),
+        serve_stacks_all_on(recv_cot_part, "tp"),
     )
     rows_in = recv_rows.reshape(-1, width)
     cot_in = recv_cot.reshape(-1, width)

time: 326 us -> 331 us (1.015)
  local copies, waits for them, and re-layouts: 4.82 us -> 12.8 us
  matrix products: 39.1 us -> 35.6 us
    reshape x0 -> x1, local copies, waits for them, and re-layouts: none -> 4.32 us  [serve_stacks_all_on(): return jnp.concatenate(taken_in, axis=2)]
    unnamed x29 -> x38, local copies, waits for them, and re-layouts: 2.68 us -> 6.33 us
    dot_general x1, matrix products: 6.74 us -> 3.35 us  [expert_grads(): lax.dot_general(cot_in, down_weight, (((1,), (1,)), ((), ())), preferred_...]
where the time goes in v1:
time: 331 us; the launch traced here: 330 us
  waiting for transfers between devices  185 us (56%)
  blocking collectives  65.5 us (20%)
  matrix products  35.6 us (11%)
  between operations  14.1 us (4%)
  local copies, waits for them, and re-layouts  12.8 us (4%)
  starting transfers between devices  11.3 us (3%)
  other arithmetic  5.65 us (2%)
    unnamed x5, waiting for transfers between devices  122 us
    reduce_scatter x1, waiting for transfers between devices, shards(): lax.psum_scatter(partial_dx.reshape(ep_count, capacity, width).astype(jnp...  33.2 us
    all_to_all x1, blocking collectives, shards(): lax.all_to_all(pack_rows(tok_part), 'ep', split_axis=0, concat_axis=0, ti...  27.3 us
    all_to_all x1, blocking collectives, shards(): lax.all_to_all(pack_rows(cot_part), 'ep', split_axis=0, concat_axis=0, ti...  23.3 us
    all_gather x1, waiting for transfers between devices, serve_stacks_all_on(): taken_in = all_gather(in_array, axis_name=shard_axis)  21.4 us
    all_to_all x1, blocking collectives, shards(): lax.all_to_all(gate_out, 'ep', split_axis=0, concat_axis=0, tiled=True)  9.04 us
  transfers between devices with their start and end apart: 6, of which 5 were waited for; matrix products, arithmetic and copies ran while one was open for 8% of the time, Pallas kernels for 0%

profile of v1, /device:TPU:0, one launch (start us, length us, event | category | flops | bytes accessed | tf_op | source)
XLA Modules:
  0.0 330.0 jit_solution(1605193063481447364)
XLA Ops:
  12.1 27.3 %all_to_all.33 = bf16[8,96,512]{2,1,0:T(8,128)(2,1)} all-to-all(bf16[8,96,512]{2,1,0:T(8,128)(2,1)S(1)} %bitcast.89), channel_id=1, replica_groups=mesh['ep'=8,'tp'=4] {'ep'}, dimensions={0} | all-to-all | bytes 1572864 | tf_op jit(solution)/shard_map/all_to_all | solution.py:105
  40.8 23.3 %all_to_all.34 = bf16[8,96,512]{2,1,0:T(8,128)(2,1)} all-to-all(bf16[8,96,512]{2,1,0:T(8,128)(2,1)S(1)} %bitcast.90), channel_id=1, replica_groups=mesh['ep'=8,'tp'=4] {'ep'}, dimensions={0} | all-to-all | bytes 1572864 | tf_op jit(solution)/shard_map/all_to_all | solution.py:106
  64.7 2.4 all-gather.4.cloned.1.call-done
  67.1 5.7 %fusion.11 = f32[768,512]{0,1:T(8,128)} fusion(bf16[768,2048]{1,0:T(8,128)(2,1)} %bitcast.104, bf16[1,2048,512]{2,1,0:T(8,128)(2,1)} %param.12), kind=kOutput, calls=%fused_computation.15 | convolution fusion | flops 1610612736 | bytes 6815744 | tf_op jit(solution)/shard_map/dot_general | solution.py:43
  72.8 3.0 fusion.8
  75.8 21.4 %all-gather.6.cloned.1.call-done = bf16[32,96,512]{2,1,0:T(8,128)(2,1)} async-done(((bf16[8,96,512]{2,1,0:T(8,128)(2,1)}), bf16[32,96,512]{2,1,0:T(8,128)(2,1)}) %all-gather.6.cloned.1.call-update) | async-done | bytes 3145744 | tf_op jit(solution)/shard_map/all_gather | solution.py:11
  97.2 4.3 %copy.94 = bf16[8,96,4,512]{3,2,1,0:T(4,128)(2,1)S(1)} copy(bf16[8,96,4,512]{3,1,0,2:T(8,128)(2,1)} %bitcast.88) | data formatting | bytes 6291456 | tf_op jit(solution)/shard_map/reshape | solution.py:12
  103.4 1.8 copy-done.15
  105.3 3.3 %multiply_reduce_fusion = (f32[768]{0:T(1024)S(1)}, bf16[768,512]{0,1:T(8,128)(2,1)}, f32[768,512]{0,1:T(8,128)}) fusion(f32[768,512]{0,1:T(8,128)S(1)} %copy-done.7, f32[768,512]{0,1:T(8,128)S(1)} %copy-done.8, bf16[768,2048]{1,0:T(8,128)(2,1)S(1)} %bitcast.86, bf16[1,512,2048]{2,1,0:T(8,128)(2,1)S(1)} %copy-done.15), kind=kOutput, calls=%fused_computation.20 | convolution fusion | flops 1614150912 | bytes 10750976 | tf_op jit(solution)/shard_map/dot_general | solution.py:44
  108.7 5.9 %psum.7 = bf16[8,96]{1,0:T(8,128)(2,1)S(1)} all-reduce(f32[8,96]{1,0:T(8,128)S(1)} %reshape.150), channel_id=1, replica_groups=mesh['ep'=8,'tp'=4] {'tp'}, use_global_device_ids=true, to_apply=%region_7.8 | all-reduce | flops 768 | bytes 4608 | tf_op jit(solution)/shard_map/psum | solution.py:132
  115.1 5.7 %all-to-all-start.4 = ((bf16[8,1,96]{2,1,0:T(2,128)(2,1)}), bf16[8,1,96]{2,1,0:T(2,128)(2,1)S(1)}, u32[]{:S(2)}, u32[]{:S(2)}) async-start(bf16[8,1,96]{2,1,0:T(2,128)(2,1)} %copy.97), calls=%async_computation.5 | async-start | bytes 8192 | tf_op jit(solution)/shard_map/all_to_all | solution.py:137
  121.1 6.1 %all-to-all-done.4 = bf16[8,1,96]{2,1,0:T(2,128)(2,1)S(1)} async-done(((bf16[8,1,96]{2,1,0:T(2,128)(2,1)}), bf16[8,1,96]{2,1,0:T(2,128)(2,1)S(1)}, u32[]{:S(2)}, u32[]{:S(2)}) %all-to-all-start.4) | async-done | bytes 1568 | tf_op jit(solution)/shard_map/all_to_all | solution.py:137
  128.0 9.0 %all_to_all.35 = bf16[8,1,96]{2,1,0:T(2,128)(2,1)S(1)} all-to-all(bf16[8,1,96]{2,1,0:T(2,128)(2,1)S(1)} %copy.93), channel_id=1, replica_groups=mesh['ep'=8,'tp'=4] {'ep'}, dimensions={0} | all-to-all | bytes 3072 | tf_op jit(solution)/shard_map/all_to_all | solution.py:107
  137.2 3.1 multiply_convert_fusion.7
  140.4 1.8 fusion.6
  142.5 3.5 %add_convert_fusion = bf16[768,2048]{1,0:T(8,128)(2,1)} fusion(f32[768,2048]{1,0:T(8,128)S(1)} %fusion.6, bf16[768,512]{0,1:T(8,128)(2,1)S(1)} %get-tuple-element.12, bf16[1,2048,512]{2,1,0:T(8,128)(2,1)S(1)} %copy-done.6), kind=kOutput, calls=%fused_computation.1 | convolution fusion | flops 1613758464 | bytes 12320768 | tf_op jit(solution)/shard_map/dot_general | solution.py:123
  146.2 1.8 fusion.31
  147.9 33.2 %reduce-scatter.5.cloned.1.call-done = bf16[8,96,512]{2,1,0:T(8,128)(2,1)} async-done(((bf16[8,96,2048]{2,1,0:T(8,128)(2,1)}), bf16[8,96,512]{2,1,0:T(8,128)(2,1)}) %reduce-scatter.5.cloned.1.call-update) | async-done | bytes 786448 | tf_op jit(solution)/shard_map/reduce_scatter | solution.py:126
  181.2 5.5 %all-to-all-start.3 = ((bf16[8,96,512]{2,1,0:T(8,128)(2,1)}), bf16[8,96,512]{2,1,0:T(8,128)(2,1)S(1)}, u32[]{:S(2)}, u32[]{:S(2)}) async-start(bf16[8,96,512]{2,1,0:T(8,128)(2,1)} %reduce-scatter.5.cloned.1.call-done), calls=%async_computation.4 | async-start | bytes 1572864 | tf_op jit(solution)/shard_map/all_to_all | solution.py:134
  186.7 5.4 %fusion.3 = bf16[1,2048,512]{2,1,0:T(8,128)(2,1)} fusion(bf16[768,2048]{1,0:T(8,128)(2,1)} %bitcast.105, bf16[768,512]{0,1:T(8,128)(2,1)} %copy-done.5), kind=kOutput, calls=%fused_computation.7 | convolution fusion | flops 1611661312 | bytes 6029312 | tf_op jit(solution)/shard_map/dot_general | solution.py:59
  192.1 3.2 fusion.5
  195.4 3.2 fusion.4
  198.6 121.6 %reduce-scatter.7.cloned.1.call-done = f32[64,4]{1,0:T(8,128)} async-done(((f32[2048,4]{1,0:T(8,128)}), f32[64,4]{1,0:T(8,128)}) %reduce-scatter.7.cloned.1.call-update) | async-done | bytes 1040
  320.2 1.4 copy.102
  (91 shorter events, 12.6 us)
Async XLA Ops:
  7.2 65.6 %copy-start = (bf16[1,2048,512]{2,1,0:T(8,128)(2,1)S(1)}, bf16[1,2048,512]{2,1,0:T(8,128)(2,1)}, u32[]{:S(2)}) copy-start(bf16[1,2048,512]{2,1,0:T(8,128)(2,1)} %param.11) | copy-start | bytes 6291460
  7.2 60.0 %all-gather.4.cloned.1.call-start = ((), (), s32[]{:S(2)}) async-start(), calls=%async_computation.7 | async-start | bytes 3932160 | tf_op jit(solution)/shard_map/all_gather | solution.py:110
  39.4 24.9 %copy-start.11 = (s32[128,2]{0,1:T(2,128)S(1)}, s32[128,2]{0,1:T(2,128)}, u32[]{:S(2)}) copy-start(s32[128,2]{0,1:T(2,128)} %param.9) | copy-start | bytes 3076
  39.5 25.0 %copy-start.9 = (bf16[128,2048]{1,0:T(8,128)(2,1)S(1)}, bf16[128,2048]{1,0:T(8,128)(2,1)}, u32[]{:S(2)}) copy-start(bf16[128,2048]{1,0:T(8,128)(2,1)} %param.7) | copy-start | bytes 1572868
  39.5 25.0 %copy-start.10 = (bf16[2048,4]{0,1:T(4,128)(2,1)S(1)}, bf16[2048,4]{0,1:T(4,128)(2,1)}, u32[]{:S(2)}) copy-start(bf16[2048,4]{0,1:T(4,128)(2,1)} %param.10) | copy-start | bytes 49156
  39.5 57.8 %all-gather.6.cloned.1.call-start = ((), (), s32[]{:S(2)}) async-start(), calls=%async_computation.9 | async-start | bytes 3932160 | tf_op jit(solution)/shard_map/all_gather | solution.py:11
  67.1 5.7 %copy-start.13 = (bf16[8,96,2048]{2,1,0:T(8,128)(2,1)S(1)}, bf16[8,96,2048]{2,1,0:T(8,128)(2,1)}, u32[]{:S(2)}) copy-start(bf16[8,96,2048]{2,1,0:T(8,128)(2,1)} %all-gather.4.cloned.1.call-done) | copy-start | bytes 9437188
  101.6 1.4 copy-start.7
  101.6 1.9 copy-start.8
  101.6 3.7 %copy-start.15 = (bf16[1,512,2048]{2,1,0:T(8,128)(2,1)S(1)}, bf16[1,512,2048]{2,1,0:T(8,128)(2,1)}, u32[]{:S(2)}) copy-start(bf16[1,512,2048]{2,1,0:T(8,128)(2,1)} %param.13) | copy-start | bytes 6291460
  102.6 6.0 %copy-start.1 = (bf16[96,8,4,512]{3,1,2,0:T(8,128)(2,1)}, bf16[96,8,4,512]{3,1,2,0:T(8,128)(2,1)S(1)}, u32[]{:S(2)}) copy-start(bf16[96,8,4,512]{3,1,2,0:T(8,128)(2,1)S(1)} %copy.104) | copy-start | bytes 9437188
  115.1 12.1 %all-to-all-start.4 = ((bf16[8,1,96]{2,1,0:T(2,128)(2,1)}), bf16[8,1,96]{2,1,0:T(2,128)(2,1)S(1)}, u32[]{:S(2)}, u32[]{:S(2)}) async-start(bf16[8,1,96]{2,1,0:T(2,128)(2,1)} %copy.97), calls=%async_computation.5 | async-start | bytes 8192 | tf_op jit(solution)/shard_map/all_to_all | solution.py:137
  120.8 60.4 %reduce-scatter.5.cloned.1.call-start = ((), (), s32[]{:S(2)}) async-start(), calls=%async_computation.8 | async-start | bytes 3932160 | tf_op jit(solution)/shard_map/reduce_scatter | solution.py:126
  127.4 12.9 %copy-start.12 = (f32[1,128,2,1]{1,0,3,2:T(1,128)}, f32[1,128,2,1]{1,0,3,2:T(1,128)S(1)}, u32[]{:S(2)}) copy-start(f32[1,128,2,1]{1,0,3,2:T(1,128)S(1)} %fusion.23) | copy-start | bytes 3076
  140.3 1.9 copy-start.5
  140.3 1.9 copy-start.3
  140.3 2.2 copy-start.6
  146.1 174.1 %reduce-scatter.7.cloned.1.call-start = ((), (), s32[]{:S(2)}) async-start(), calls=%async_computation.10 | async-start | bytes 1081344
  181.2 140.4 %all-to-all-start.3 = ((bf16[8,96,512]{2,1,0:T(8,128)(2,1)}), bf16[8,96,512]{2,1,0:T(8,128)(2,1)S(1)}, u32[]{:S(2)}, u32[]{:S(2)}) async-start(bf16[8,96,512]{2,1,0:T(8,128)(2,1)} %reduce-scatter.5.cloned.1.call-done), calls=%async_computation.4 | async-start | bytes 1572864 | tf_op jit(solution)/shard_map/all_to_all | solution.py:134
  186.7 5.4 %copy-start.2 = (bf16[96,8,4,512]{3,1,2,0:T(8,128)(2,1)S(1)}, bf16[96,8,4,512]{3,1,2,0:T(8,128)(2,1)}, u32[]{:S(2)}) copy-start(bf16[96,8,4,512]{3,1,2,0:T(8,128)(2,1)} %copy-done.1) | copy-start | bytes 9437188
  186.7 5.4 %copy-start.16 = (bf16[768,512]{0,1:T(8,128)(2,1)S(1)}, bf16[768,512]{0,1:T(8,128)(2,1)}, u32[]{:S(2)}) copy-start(bf16[768,512]{0,1:T(8,128)(2,1)} %get-tuple-element.11) | copy-start | bytes 2359300
  192.1 3.3 copy-start.4
  192.1 3.3 copy-start.14
Sparse Core Ops, SparseCore 0:
  39.6 27.5 all-gather.3
  68.7 28.4 all-gather.5
  146.2 34.9 reduce-scatter.4
  183.3 136.8 reduce-scatter.6
